TPU v7x, 128 devices: a whole 4x4x4 slice. The times are simulated.
128 devices in a mesh: sp: 16 (over z, y), tp: 4 (over x), dp: 2 (over core).
Axes of the slice: x: 4, y: 4, z: 4, core: 2. Of those that a mesh axis runs over, the one named last changes fastest.
Arguments:
- latent: bfloat16 [2, 12288, 2048], P('dp', ('sp', 'tp')), may hold values from -3 to 3
- cond: bfloat16 [2, 2048], P('dp', 'sp'), may hold values from -6 to 6
- cond_ctx: bfloat16 [2048], P('sp'), may hold values from -6 to 6
- context: bfloat16 [2, 512, 2048], P('dp', 'sp'), may hold values from -6 to 6
- norm_gain: bfloat16 [2048], replicated, may hold values from 0.099609375 to 1.8984375
- mod_shift: bfloat16 [2048, 2048], P('sp', 'tp'), may hold values from -0.125 to 0.125
- mod_scale: bfloat16 [2048, 2048], P('sp', 'tp'), may hold values from -0.125 to 0.125
- mod_gate: bfloat16 [2048, 2048], P('sp', 'tp'), may hold values from -0.125 to 0.125
- w_query: bfloat16 [2048, 1024], P(None, 'tp'), may hold values from -0.125 to 0.125
- w_key: bfloat16 [2048, 256], P(None, 'tp'), may hold values from -0.125 to 0.125
- w_value: bfloat16 [2048, 256], P(None, 'tp'), may hold values from -0.125 to 0.125
- q_gain: bfloat16 [64], replicated, may hold values from 1 to 5.5
- k_gain: bfloat16 [64], replicated, may hold values from 1 to 5.5
- ctx_lift: float32 [16], P('tp'), may hold values from 1 to 3
- w_out: bfloat16 [1024, 2048], replicated, may hold values from -1.5 to 1.5
Outputs:
- mixed: bfloat16 [2, 12288, 2048], P('dp', ('sp', 'tp'))
All inputs are finite; a program needn't handle non-finite values.
Results may differ from a plain program's by a relative error of at most 0.009.
The roundings to bfloat16 on the way count: a program that leaves them out, or rounds other values in their place, can miss the bound.
Values may be sent and summed in bfloat16 or wider, within the bound.
A program may use at most 64 MiB of HBM per device.

v0:
```python
import functools

import jax
import jax.numpy as jnp
import numpy as np
from jax import lax
from jax.experimental import pallas as pl
from jax.experimental.pallas import tpu as pltpu
from jax.sharding import PartitionSpec as P

HD = 64
GRID_W = 128
EPS = 1e-06
THETA = 10000.0
MESH = pl.DeviceIdType.MESH
LOG2E = 1.4426950408889634
QB = 256
KB = 256


def rope_tables(grid_rows):
    n = HD // 4
    inverse = (np.float32(THETA) ** (-np.arange(n, dtype=np.float32) / np.float32(n))).astype(np.float32)

    def table(count, low):
        angles = (np.arange(count, dtype=np.float32)[:, None] * inverse).astype(np.float32)
        zero = np.zeros((count, 2 * n), np.float32)
        sign = np.tile(np.array([-1.0, 1.0], np.float32), n)
        c = np.repeat(np.cos(angles.astype(np.float64)), 2, axis=1).astype(np.float32)
        s = np.repeat(np.sin(angles.astype(np.float64)), 2, axis=1).astype(np.float32) * sign
        parts = ([c, zero], [s, zero]) if low else ([zero, c], [zero, s])
        return [np.tile(np.concatenate(p, axis=1), (1, 2)) for p in parts]

    return np.stack(table(grid_rows, True)), np.stack(table(GRID_W, False))


def kernel(
    n_sp, n_tp, group,
    latent, cond, cond_ctx, norm_gain, q_gain, k_gain, lift, row_tab, col_tab,
    context_h, mshift_h, mscale_h, mgate_h, wq_h, wk_h, wv_h, wout_h,
    out,
    context, mods_w, wq, wk, wv, wkv, wout,
    raw, part, part_in, mods_all, ab, rope, q_tok, q_t, kv_all, kv_ctx, v_t, s_a, s_b, acc, m_st, o_tok, o_all,
    local_sem, lat_send, lat_recv, pa_send, pa_recv, pb_send, pb_recv, kv_send, kv_recv, o_ssem, o_rsem,
):
    rows = latent.shape[0]
    half = rows // 2
    width = latent.shape[1]
    chunk = width // n_tp
    tokens = rows * n_tp
    ctx_rows = context.shape[0]
    sp = lax.axis_index("sp")
    tp = lax.axis_index("tp")
    tx, ty = tp % 2, tp // 2
    peers = (ty * 2 + (1 - tx), (1 - ty) * 2 + tx, (1 - ty) * 2 + (1 - tx))
    sp_order = sorted(range(1, n_sp), key=lambda d: min(d, n_sp - d))

    local = [
        pltpu.make_async_copy(src, dst, local_sem.at[i])
        for i, (src, dst) in enumerate(
            (
                (mshift_h, mods_w.at[0]),
                (mscale_h, mods_w.at[1]),
                (mgate_h, mods_w.at[2]),
                (context_h, context),
                (wk_h, wk),
                (wv_h, wv),
                (wq_h, wq),
                (wout_h, wout),
            )
        )
    ]
    for copy in local:
        copy.start()

    barrier = pltpu.get_barrier_semaphore()
    for peer in peers:
        pl.semaphore_signal(barrier, inc=1, device_id={"tp": peer}, device_id_type=MESH)
    for d in range(1, n_sp):
        pl.semaphore_signal(barrier, inc=1, device_id={"sp": (sp + d) % n_sp}, device_id_type=MESH)
    pl.semaphore_wait(barrier, n_tp - 1 + n_sp - 1)

    def send(src, dst, ssem, rsem, device):
        return pltpu.make_async_remote_copy(
            src_ref=src, dst_ref=dst, send_sem=ssem, recv_sem=rsem, device_id=device, device_id_type=MESH
        )

    top, low = pl.ds(0, half), pl.ds(half, half)
    lat = []

    def send_rows(index, src, slot, piece, peer):
        copy = send(src, raw.at[slot, piece], lat_send.at[index], lat_recv.at[index], {"tp": peer})
        copy.start()
        lat.append(copy)

    send_rows(0, latent.at[top], 0, top, peers[0])
    send_rows(1, latent.at[low], 1, low, peers[1])
    send_rows(2, latent.at[low], 0, low, peers[0])
    send_rows(3, latent.at[top], 1, top, peers[1])

    act = jnp.concatenate([cond[...], cond_ctx[...]], axis=0).astype(jnp.float32)
    act = (act / (1.0 + jnp.exp(-act))).astype(jnp.bfloat16)
    act = jnp.concatenate([act, jnp.zeros((14, act.shape[1]), jnp.bfloat16)], axis=0)
    for i in range(3):
        local[i].wait()
    sums = [jnp.dot(act, mods_w[i], preferred_element_type=jnp.float32)[0:2] for i in range(3)]
    part[...] = jnp.concatenate(sums + [jnp.zeros((2, chunk), jnp.float32)], axis=0)
    pa = []
    for d in sp_order:
        copy = send(part, part_in.at[d - 1], pa_send.at[d - 1], pa_recv.at[d - 1], {"sp": (sp + d) % n_sp})
        copy.start()
        pa.append(copy)

    groups = tokens // GRID_W
    for i in range(2):
        for g in range(groups):
            rope[i, pl.ds(g * GRID_W, GRID_W), :] = (
                row_tab[i, pl.ds(sp * groups + g, 1), :] + col_tab[i, :, :]
            )
    local[4].wait()
    local[5].wait()
    wkv[...] = jnp.concatenate([wk[...], wv[...]], axis=1)

    total = part[...]
    for copy in pa:
        copy.wait_recv()
    for d in range(1, n_sp):
        total = total + part_in[d - 1]
    mods_all[tp] = total
    pb = []
    for i, peer in enumerate(peers):
        copy = send(mods_all.at[tp], mods_all.at[tp], pb_send.at[i], pb_recv.at[i], {"tp": peer})
        copy.start()
        pb.append(copy)
    lat[0].wait_recv()
    send_rows(4, raw.at[0, top], 2, top, peers[1])
    lat[1].wait_recv()
    send_rows(5, raw.at[1, low], 2, low, peers[0])

    for copy in pb:
        copy.wait_recv()
    gain = norm_gain[...].astype(jnp.float32)
    for j in range(n_tp):
        cols = pl.ds(j * chunk, chunk)
        block = mods_all[j]
        ab[0:2, cols] = gain[:, j * chunk : (j + 1) * chunk] * (1.0 + block[2:4])
        ab[2:4, cols] = block[0:2]

    lane = lax.broadcasted_iota(jnp.int32, (1, 2 * HD), 1)
    even = lane % 2 == 0
    left = lane < HD
    ones = (
        (lax.broadcasted_iota(jnp.int32, (2 * HD, 2 * HD), 0) < HD)
        == (lax.broadcasted_iota(jnp.int32, (2 * HD, 2 * HD), 1) < HD)
    ).astype(jnp.bfloat16)
    qg = jnp.concatenate([q_gain[...]] * 2, axis=1).astype(jnp.float32)
    kg = jnp.concatenate([k_gain[...]] * 2, axis=1).astype(jnp.float32)

    def modulated(block, row):
        values = block.astype(jnp.float32)
        scale = lax.rsqrt(jnp.mean(values * values, axis=-1, keepdims=True) + EPS)
        return (values * scale * ab[row : row + 1, :] + ab[row + 2 : row + 3, :]).astype(jnp.bfloat16)

    def headed(x, g):
        square = x * x
        high = square.astype(jnp.bfloat16)
        rest = (square - high.astype(jnp.float32)).astype(jnp.bfloat16)
        mean = (
            jnp.dot(high, ones, preferred_element_type=jnp.float32)
            + jnp.dot(rest, ones, preferred_element_type=jnp.float32)
        ) * (1.0 / HD)
        return x * lax.rsqrt(mean + EPS) * g

    def turned(x, cosine, sine):
        partner = jnp.where(even, pltpu.roll(x, 2 * HD - 1, 1), pltpu.roll(x, 1, 1))
        return x * cosine + partner * sine

    factor = LOG2E * HD ** (-0.5)

    def absorb_rows(block, owner):
        u = modulated(block, 0)
        where = pl.ds(pl.multiple_of(owner * rows, rows), rows)
        cosine, sine = rope[0, where, :], rope[1, where, :]
        kv = jnp.dot(u, wkv[...], preferred_element_type=jnp.float32)
        keys = turned(headed(kv, kg), cosine, sine)
        kv_all[0, where, :] = jnp.where(left, keys, kv).astype(jnp.bfloat16)
        raw_q = jnp.dot(u, wq[...], preferred_element_type=jnp.float32)
        for pair in range(group // 2):
            x = raw_q[:, pair * 2 * HD : (pair + 1) * 2 * HD]
            x = turned(headed(x, qg), cosine, sine).astype(jnp.bfloat16)
            q_tok[pair, where, :] = x.astype(jnp.float32) * factor

    local[3].wait()
    uc = modulated(context[...], 1)
    kvc = jnp.dot(uc, wkv[...], preferred_element_type=jnp.float32)
    kv_all[0, pl.ds(tokens, ctx_rows), :] = jnp.where(left, headed(kvc, kg), kvc).astype(jnp.bfloat16)
    local[6].wait()
    absorb_rows(latent[...], tp)
    lat[2].wait_recv()
    absorb_rows(raw[0], peers[0])
    lat[3].wait_recv()
    absorb_rows(raw[1], peers[1])
    lat[4].wait_recv()
    lat[5].wait_recv()
    absorb_rows(raw[2], peers[2])

    kvs = {}
    for d in sp_order:
        copy = send(kv_all.at[0], kv_all.at[d], kv_send.at[d - 1], kv_recv.at[d - 1], {"sp": (sp + d) % n_sp})
        copy.start()
        kvs[d] = copy

    blocks = tokens // QB
    for pair in range(group // 2):
        for tb in range(blocks):
            t = q_tok[pair, tb * QB : (tb + 1) * QB, :].T
            high = t.astype(jnp.bfloat16)
            rest = (t - high.astype(jnp.float32)).astype(jnp.bfloat16)
            none = jnp.zeros((HD, QB), jnp.bfloat16)
            for j in range(2):
                cut = slice(j * HD, (j + 1) * HD)
                q_t[tb * group + 2 * pair + j] = jnp.concatenate([high[cut], none, rest[cut], none], axis=0)
    v_t[HD:, :] = jnp.ones((v_t.shape[0] - HD, tokens), jnp.bfloat16)
    acc[...] = jnp.zeros_like(acc)
    m_st[...] = jnp.full(m_st.shape, -1e30, jnp.float32)
    n_q = blocks * group
    bufs = (s_a, s_b)

    def sweep(load, n_keys, lifted, done):
        chunks = n_keys // KB

        def scores(b, c, dst, top):
            piece = load(c)
            s = jnp.dot(
                jnp.concatenate([piece, piece], axis=1), q_t[b], preferred_element_type=jnp.float32
            )
            if lifted:
                s = s + lift[b % group] * LOG2E
            dst[c * KB : (c + 1) * KB, :] = s
            high = jnp.max(s.reshape(KB // 8, 8, QB), axis=0)
            return high if top is None else jnp.maximum(top, high)

        top = None
        for c in range(chunks):
            top = scores(0, c, bufs[0], top)
        for b in range(n_q):
            cur, nxt = bufs[b % 2], bufs[(b + 1) % 2]
            m_old = m_st[b]
            m = jnp.maximum(m_old, jnp.max(top, axis=0, keepdims=True))
            m_st[b] = m
            alpha = jnp.exp2(m_old - m)
            top, o = None, None
            for c in range(chunks):
                if b + 1 < n_q:
                    top = scores(b + 1, c, nxt, top)
                x = cur[c * KB : (c + 1) * KB, :].reshape(KB // 8, 8, QB) - m[None]
                p = jnp.exp2(x).reshape(KB, QB).astype(jnp.bfloat16)
                term = jnp.dot(v_t[:, c * KB : (c + 1) * KB], p, preferred_element_type=jnp.float32)
                o = term if o is None else o + term
            o = acc[b] * alpha[0:1] + o
            if done is None:
                acc[b] = o
            else:
                done(b, o)

    def kv_copy(d):
        return send(kv_all.at[0], kv_all.at[d], kv_send.at[d - 1], kv_recv.at[d - 1], {"sp": (sp + d) % n_sp})

    def slot_step(step, carry):
        d = jnp.where(step % 2 == 1, (step + 1) // 2, (n_sp - step // 2) % n_sp)

        @pl.when(step > 0)
        def _():
            kv_copy(d).wait_recv()

        kv_ctx[pl.ds(pl.multiple_of(step * ctx_rows, ctx_rows), ctx_rows), :] = kv_all[d, tokens:, :]
        for c in range(tokens // KB):
            v_t[:HD, c * KB : (c + 1) * KB] = kv_all[d, c * KB : (c + 1) * KB, :].T[HD:]
        sweep(lambda c: kv_all[d, c * KB : (c + 1) * KB, :], tokens, False, None)
        return carry

    lax.fori_loop(0, n_sp, slot_step, 0)

    finished = {}

    def done(b, o):
        finished[b % group] = (o[:HD] / o[HD : HD + 1]).astype(jnp.bfloat16).astype(jnp.float32)
        if b % group == group - 1:
            tb = b // group
            for pair in range(group // 2):
                both = jnp.concatenate([finished[2 * pair], finished[2 * pair + 1]], axis=0)
                o_tok[tb * QB : (tb + 1) * QB, pair * 2 * HD : (pair + 1) * 2 * HD] = both.T.astype(jnp.bfloat16)

    n_ctx = n_sp * ctx_rows
    for c in range(n_ctx // KB):
        v_t[:HD, c * KB : (c + 1) * KB] = kv_ctx[c * KB : (c + 1) * KB, :].T[HD:]
    sweep(lambda c: kv_ctx[c * KB : (c + 1) * KB, :], n_ctx, True, done)

    span = group * HD
    mine = pl.ds(pl.multiple_of(tp * span, span), span)
    o_copies = []
    for i, owner in enumerate(peers):
        where = pl.ds(pl.multiple_of(owner * rows, rows), rows)
        copy = send(o_tok.at[where], o_all.at[:, mine], o_ssem.at[i], o_rsem.at[i], {"tp": owner})
        copy.start()
        o_copies.append(copy)
    o_all[:, mine] = o_tok[pl.ds(pl.multiple_of(tp * rows, rows), rows), :]
    local[7].wait()
    for copy in o_copies:
        copy.wait_recv()

    for j in range(n_tp):
        cols = pl.ds(j * chunk, chunk)
        y = jnp.dot(o_all[...], wout[:, cols], preferred_element_type=jnp.float32)
        gate = mods_all[j, 4:5, :]
        out[:, cols] = (latent[:, cols].astype(jnp.float32) + gate * y).astype(jnp.bfloat16)

    for copy in lat + pa + pb + list(kvs.values()) + o_copies:
        copy.wait_send()


def on_device(n_sp, n_tp, latent, cond, cond_ctx, context, norm_gain, mod_shift, mod_scale, mod_gate,
              w_query, w_key, w_value, q_gain, k_gain, ctx_lift, w_out):
    _, rows, width = latent.shape
    tokens = rows * n_tp
    ctx_rows = context.shape[1]
    group = w_query.shape[1] // w_key.shape[1]
    keys = tokens + ctx_rows
    row_tab, col_tab = rope_tables(tokens * n_sp // GRID_W)
    chunk = mod_shift.shape[1]
    n_q = tokens // QB * group
    bf, f32 = jnp.bfloat16, jnp.float32
    vmem = pl.BlockSpec(memory_space=pltpu.VMEM)
    smem = pl.BlockSpec(memory_space=pltpu.SMEM)
    hbm = pl.BlockSpec(memory_space=pl.ANY)
    dma = pltpu.SemaphoreType.DMA
    out = pl.pallas_call(
        functools.partial(kernel, n_sp, n_tp, group),
        out_shape=jax.ShapeDtypeStruct((rows, width), bf),
        in_specs=[vmem] * 6 + [smem] + [vmem] * 2 + [hbm] * 8,
        out_specs=vmem,
        scratch_shapes=[
            pltpu.VMEM((ctx_rows, width), bf),
            pltpu.VMEM((3,) + mod_shift.shape, bf),
            pltpu.VMEM(w_query.shape, bf),
            pltpu.VMEM(w_key.shape, bf),
            pltpu.VMEM(w_value.shape, bf),
            pltpu.VMEM((width, 2 * HD), bf),
            pltpu.VMEM(w_out.shape, bf),
            pltpu.VMEM((n_tp - 1, rows, width), bf),
            pltpu.VMEM((8, chunk), f32),
            pltpu.VMEM((n_sp - 1, 8, chunk), f32),
            pltpu.VMEM((n_tp, 8, chunk), f32),
            pltpu.VMEM((8, width), f32),
            pltpu.VMEM((2, tokens, 2 * HD), f32),
            pltpu.VMEM((group // 2, tokens, 2 * HD), f32),
            pltpu.VMEM((n_q, 4 * HD, QB), bf),
            pltpu.VMEM((n_sp, keys, 2 * HD), bf),
            pltpu.VMEM((n_sp * ctx_rows, 2 * HD), bf),
            pltpu.VMEM((HD + 16, tokens), bf),
            pltpu.VMEM((tokens, QB), f32),
            pltpu.VMEM((tokens, QB), f32),
            pltpu.VMEM((n_q, HD + 16, QB), f32),
            pltpu.VMEM((n_q, 8, QB), f32),
            pltpu.VMEM((tokens, group * HD), bf),
            pltpu.VMEM((rows, n_tp * group * HD), bf),
            dma((8,)),
            dma((6,)), dma((6,)),
            dma((n_sp - 1,)), dma((n_sp - 1,)),
            dma((n_tp - 1,)), dma((n_tp - 1,)),
            dma((n_sp - 1,)), dma((n_sp - 1,)),
            dma((n_tp - 1,)), dma((n_tp - 1,)),
        ],
        compiler_params=pltpu.CompilerParams(
            collective_id=0, has_side_effects=True, vmem_limit_bytes=60 * 1024 * 1024
        ),
    )(
        latent[0], cond, cond_ctx[None], norm_gain[None], q_gain[None], k_gain[None], ctx_lift,
        jnp.asarray(row_tab), jnp.asarray(col_tab),
        context[0], mod_shift, mod_scale, mod_gate, w_query, w_key, w_value, w_out,
    )
    return out[None]


def solution(mesh):
    placed = (
        P("dp", ("sp", "tp"), None),
        P("dp", "sp"),
        P("sp"),
        P("dp", "sp", None),
        P(),
        P("sp", "tp"),
        P("sp", "tp"),
        P("sp", "tp"),
        P(None, "tp"),
        P(None, "tp"),
        P(None, "tp"),
        P(),
        P(),
        P("tp"),
        P(),
    )
    return jax.shard_map(
        functools.partial(on_device, mesh.shape["sp"], mesh.shape["tp"]),
        mesh=mesh,
        in_specs=placed,
        out_specs=P("dp", ("sp", "tp"), None),
        check_vma=False,
    )
```

profile of v0, /device:TPU:0, one launch (start us, length us, event | category | flops | bytes accessed | tf_op | source)
XLA Modules:
  0.0 141.5 jit_solution(8344553041995510947)
XLA Ops:
  0.0 1.3 broadcast_in_dim.16.norm_gain
  1.3 2.0 %copy.18.wk_h = bf16[2048,64]{1,0:T(8,128)(2,1)} copy(bf16[2048,64]{0,1:T(8,128)(2,1)} %param.26) | data formatting | bytes 524288 | tf_op args[9]
  3.2 2.0 %copy.19.wv_h = bf16[2048,64]{1,0:T(8,128)(2,1)} copy(bf16[2048,64]{0,1:T(8,128)(2,1)} %param.27) | data formatting | bytes 524288 | tf_op args[10]
  5.2 134.2 %shard_map.163 = bf16[192,2048]{1,0:T(8,128)(2,1)} custom-call(bf16[192,2048]{1,0:T(8,128)(2,1)} %bitcast.7, bf16[1,128]{1,0:T(2,128)(2,1)} %cond.1, bf16[1,128]{1,0:T(2,128)(2,1)} %bitcast.9, bf16[1,2048]{1,0:T(2,128)(2,1)} %broadcast_in_dim.16.norm_gain, bf16[1,64]{1,0:T(2,128)(2,1)} %bitcast.10, bf16[1,64]{1,0:T(2,128)(2,1)} %bitcast.11, f32[4]{0:T(128)} %lift.1, ...), custom_call_target="tpu_custom_call" | custom-call | tf_op jit(solution)/shard_map/pallas_call | solution.py:337
  139.4 2.1 %copy.21 = bf16[1,192,2048]{2,1,0:T(8,128)(2,1)} copy(bf16[1,192,2048]{2,1,0:T(8,128)(2,1)} %bitcast.6) | data formatting | bytes 1572864
where the time goes:
time: 143 us; the launch traced here: 142 us
  Pallas kernels  134 us (94%)
  local copies, waits for them, and re-layouts  7.29 us (5%)
    pallas_call x1, Pallas kernels, on_device(): pl.pallas_call(functools.partial(kernel, n_sp, n_tp, group), out_shape=ja...  134 us
    unnamed x3, local copies, waits for them, and re-layouts  6 us

commit v1 on v0

v1 whole, which is shorter than its diff:
```python
import functools

import jax
import jax.numpy as jnp
import numpy as np
from jax import lax
from jax.experimental import pallas as pl
from jax.experimental.pallas import tpu as pltpu
from jax.sharding import PartitionSpec as P

HD = 64
GRID_W = 128
EPS = 1e-06
THETA = 10000.0
MESH = pl.DeviceIdType.MESH
LOG2E = 1.4426950408889634
QB = 256
KB = 256
TILE = 128

PAIRS = (
    ((0, 0), (3, 0)), ((1, 0), (0, 3)), ((0, 1), (2, 0)), ((3, 3), (3, 1)),
    ((1, 3), (1, 1)), ((2, 3), (2, 1)), ((0, 2), (3, 2)), ((1, 2), (2, 2)),
)
ONWARD = {
    (0, 0): ((0, 1, (3, 0)), (0, -1, (1, 0)), (1, 1, (0, 3)), (1, -1, (0, 1))),
    (3, 0): ((0, 1, (2, 0)), (1, 1, (3, 3)), (1, -1, (3, 1))),
    (1, 0): ((1, 1, (1, 3)), (1, -1, (1, 1))),
    (2, 0): ((1, 1, (2, 3)), (1, -1, (2, 1))),
    (0, 3): ((1, 1, (0, 2)),),
    (1, 3): ((1, 1, (1, 2)),),
    (3, 1): ((1, -1, (3, 2)),),
    (2, 1): ((1, -1, (2, 2)),),
}


def slot_of(place):
    return place[0] * 4 + place[1]


def pick(step, values):
    chosen = values[0]
    for i, value in enumerate(values[1:], 1):
        chosen = jnp.where(step == i, value, chosen)
    return chosen


def rope_tables(grid_rows):
    n = HD // 4
    inverse = (np.float32(THETA) ** (-np.arange(n, dtype=np.float32) / np.float32(n))).astype(np.float32)

    def table(count, low):
        angles = (np.arange(count, dtype=np.float32)[:, None] * inverse).astype(np.float32)
        zero = np.zeros((count, 2 * n), np.float32)
        sign = np.tile(np.array([-1.0, 1.0], np.float32), n)
        c = np.repeat(np.cos(angles.astype(np.float64)), 2, axis=1).astype(np.float32)
        s = np.repeat(np.sin(angles.astype(np.float64)), 2, axis=1).astype(np.float32) * sign
        parts = ([c, zero], [s, zero]) if low else ([zero, c], [zero, s])
        return [np.tile(np.concatenate(p, axis=1), (1, 2)) for p in parts]

    return np.stack(table(grid_rows, True)), np.stack(table(GRID_W, False))


def kernel(
    n_sp, n_tp, group,
    latent, cond, cond_ctx, norm_gain, q_gain, k_gain, lift, row_tab, col_tab,
    context_h, mshift_h, mscale_h, mgate_h, wq_h, wk_h, wv_h, wout_h,
    out,
    context, mods_w, wq, wkv, wout,
    raw, part, part_in, mods_all, ab, rope, u_buf, q_t, kv1, kv2, kv_ctx, v_t, s_a, s_b, acc, m_st, o_tok, o_all,
    local_sem, lat_send, lat_recv, pa_send, pa_recv, pb_send, pb_recv, kv_send, kv_recv, o_ssem, o_rsem,
):
    rows = latent.shape[0]
    half = rows // 2
    width = latent.shape[1]
    chunk = width // n_tp
    tokens = rows * n_tp
    share = tokens // 2
    ctx_rows = context.shape[0]
    sp = lax.axis_index("sp")
    tp = lax.axis_index("tp")
    dp = lax.axis_index("dp")
    left_tp, right_tp, far_tp = (tp + n_tp - 1) % n_tp, (tp + 1) % n_tp, (tp + 2) % n_tp
    peers = (left_tp, right_tp, far_tp)
    sp_order = sorted(range(1, n_sp), key=lambda d: min(d, n_sp - d))

    local = [
        pltpu.make_async_copy(src, dst, local_sem.at[i])
        for i, (src, dst) in enumerate(
            (
                (mshift_h, mods_w.at[0]),
                (mscale_h, mods_w.at[1]),
                (mgate_h, mods_w.at[2]),
                (context_h, context),
                (wk_h, wkv.at[0:HD]),
                (wv_h, wkv.at[HD : 2 * HD]),
                (wq_h, wq),
                (wout_h, wout),
            )
        )
    ]
    for copy in local:
        copy.start()

    barrier = pltpu.get_barrier_semaphore()
    for peer in peers:
        pl.semaphore_signal(barrier, inc=1, device_id={"tp": peer}, device_id_type=MESH)
    for d in range(1, n_sp):
        pl.semaphore_signal(barrier, inc=1, device_id={"sp": (sp + d) % n_sp}, device_id_type=MESH)
    pl.semaphore_wait(barrier, n_tp - 1 + n_sp - 1)

    def send(src, dst, ssem, rsem, device):
        return pltpu.make_async_remote_copy(
            src_ref=src, dst_ref=dst, send_sem=ssem, recv_sem=rsem, device_id=device, device_id_type=MESH
        )

    top, low = pl.ds(0, half), pl.ds(half, half)
    lat = []

    def send_rows(index, src, slot, piece, peer):
        copy = send(src, raw.at[slot, piece], lat_send.at[index], lat_recv.at[index], {"tp": peer})
        copy.start()
        lat.append(copy)

    send_rows(0, latent.at[top], 0, top, right_tp)
    send_rows(1, latent.at[top], 1, top, left_tp)

    act = jnp.concatenate([cond[...], cond_ctx[...]], axis=0).astype(jnp.float32)
    act = (act / (1.0 + jnp.exp(-act))).astype(jnp.bfloat16)
    act = jnp.concatenate([act, jnp.zeros((14, act.shape[1]), jnp.bfloat16)], axis=0)
    for i in range(3):
        local[i].wait()
    sums = [jnp.dot(act, mods_w[i], preferred_element_type=jnp.float32)[0:2] for i in range(3)]
    part[...] = jnp.concatenate(sums + [jnp.zeros((2, chunk), jnp.float32)], axis=0)
    pa = []
    for d in sp_order:
        copy = send(part, part_in.at[d - 1], pa_send.at[d - 1], pa_recv.at[d - 1], {"sp": (sp + d) % n_sp})
        copy.start()
        pa.append(copy)

    groups = tokens // GRID_W
    for i in range(2):
        for g in range(groups):
            rope[i, pl.ds(g * GRID_W, GRID_W), :] = (
                row_tab[i, pl.ds(sp * groups + g, 1), :] + col_tab[i, :, :]
            )

    total = part[...]
    for copy in pa:
        copy.wait_recv()
    for d in range(1, n_sp):
        total = total + part_in[d - 1]
    mods_all[tp] = total
    pb = []
    for i, peer in enumerate((far_tp, left_tp, right_tp)):
        copy = send(mods_all.at[tp], mods_all.at[tp], pb_send.at[i], pb_recv.at[i], {"tp": peer})
        copy.start()
        pb.append(copy)
    send_rows(2, latent.at[low], 0, low, right_tp)
    send_rows(3, latent.at[low], 1, low, left_tp)

    for i, peer in enumerate((far_tp, left_tp, right_tp)):
        pb[i].wait_recv()
    for j in range(n_tp):
        block = mods_all[j]
        for i in range(chunk // TILE):
            at = j * chunk + i * TILE
            gain = norm_gain[at // TILE : at // TILE + 1, :].astype(jnp.float32)
            ab[0:2, at : at + TILE] = gain * (1.0 + block[2:4, i * TILE : (i + 1) * TILE])
        ab[2:4, pl.ds(j * chunk, chunk)] = block[0:2]

    lane = lax.broadcasted_iota(jnp.int32, (1, 2 * HD), 1)
    even = lane % 2 == 0
    left = lane < HD
    ones = (
        (lax.broadcasted_iota(jnp.int32, (2 * HD, 2 * HD), 0) < HD)
        == (lax.broadcasted_iota(jnp.int32, (2 * HD, 2 * HD), 1) < HD)
    ).astype(jnp.bfloat16)
    qg = jnp.concatenate([q_gain[...]] * 2, axis=1).astype(jnp.float32)
    kg = jnp.concatenate([k_gain[...]] * 2, axis=1).astype(jnp.float32)
    factor = LOG2E * HD ** (-0.5)

    def modulated(block, row):
        values = block.astype(jnp.float32)
        scale = lax.rsqrt(jnp.mean(values * values, axis=-1, keepdims=True) + EPS)
        return (values * scale * ab[row : row + 1, :] + ab[row + 2 : row + 3, :]).astype(jnp.bfloat16)

    def headed(x, g):
        square = x * x
        high = square.astype(jnp.bfloat16)
        rest = (square - high.astype(jnp.float32)).astype(jnp.bfloat16)
        mean = (
            jnp.dot(high, ones, preferred_element_type=jnp.float32)
            + jnp.dot(rest, ones, preferred_element_type=jnp.float32)
        ) * (1.0 / HD)
        return x * lax.rsqrt(mean + EPS) * g

    def turned(x, cosine, sine):
        partner = jnp.where(even, pltpu.roll(x, 2 * HD - 1, 1), pltpu.roll(x, 1, 1))
        return x * cosine + partner * sine

    def key_value(u):
        return lax.dot_general(u, wkv[...], (((1,), (1,)), ((), ())), preferred_element_type=jnp.float32)

    def angles(owner, start, count):
        where = pl.ds(pl.multiple_of(owner * rows + start, half), count)
        return rope[0, where, :], rope[1, where, :]

    def absorb_keys(block, owner, start, kv, offset):
        count = block.shape[0]
        u = modulated(block, 0)
        u_buf[offset : offset + count, :] = u
        cosine, sine = angles(owner, start, count)
        x = key_value(u)
        kv[0, offset : offset + count, :] = jnp.where(
            left, turned(headed(x, kg), cosine, sine), x
        ).astype(jnp.bfloat16)

    def absorb_queries(pieces, first):
        tables = [angles(*piece) for piece in pieces]
        cosine = jnp.concatenate([t[0] for t in tables], axis=0)
        sine = jnp.concatenate([t[1] for t in tables], axis=0)
        raw_q = jnp.dot(u_buf[...], wq[...], preferred_element_type=jnp.float32)
        none = jnp.zeros((HD, QB), jnp.bfloat16)
        for pair in range(group // 2):
            x = raw_q[:, pair * 2 * HD : (pair + 1) * 2 * HD]
            x = turned(headed(x, qg), cosine, sine).astype(jnp.bfloat16).astype(jnp.float32) * factor
            for tile in range(tiles):
                t = x[tile * TILE : (tile + 1) * TILE, :].T
                t = jnp.concatenate([t[:HD], t[HD:]], axis=1)
                high = t.astype(jnp.bfloat16)
                rest = (t - high.astype(jnp.float32)).astype(jnp.bfloat16)
                q_t[first + pair * tiles + tile] = jnp.concatenate([high, none, rest, none], axis=0)

    side = int(round(n_sp ** 0.5))
    y, z = sp % side, sp // side

    def neighbour(axis, step):
        along_y = z * side + (y + step + side) % side
        along_z = (z + step + side) % side * side + y
        return jnp.where(dp == axis, along_y, along_z)

    flights = [(place, hop) for place in ONWARD for hop in ONWARD[place]]

    def flight(index, which, kv):
        place, (axis, step, target) = flights[index]
        return send(
            kv.at[slot_of(place)], kv.at[slot_of(target)],
            kv_send.at[which, index], kv_recv.at[which, slot_of(target)],
            {"sp": neighbour(axis, step)},
        )

    def pass_on(place, which, kv):
        for index in range(len(flights)):
            if flights[index][0] == place:
                flight(index, which, kv).start()

    def arrived(place, which, kv):
        for index in range(len(flights)):
            if flights[index][1][2] == place:
                flight(index, which, kv).wait_recv()

    tiles = share // TILE
    n_half = tiles * group // 2
    bufs = (s_a, s_b)

    def sweep(load, n_keys, order, lifted, done):
        chunks = n_keys // KB

        def scores(b, c, dst, top):
            piece = load(c)
            s = jnp.dot(
                jnp.concatenate([piece, piece], axis=1), q_t[b], preferred_element_type=jnp.float32
            )
            if lifted:
                pair = b % n_half // tiles
                wide = lax.broadcasted_iota(jnp.int32, (1, QB), 1)
                s = s + jnp.where(wide < TILE, lift[2 * pair], lift[2 * pair + 1]) * LOG2E
            dst[c * KB : (c + 1) * KB, :] = s
            high = jnp.max(s.reshape(KB // 8, 8, QB), axis=0)
            return high if top is None else jnp.maximum(top, high)

        top = None
        for c in range(chunks):
            top = scores(order[0], c, bufs[0], top)
        for i, b in enumerate(order):
            cur, nxt = bufs[i % 2], bufs[(i + 1) % 2]
            m_old = m_st[b]
            m = jnp.maximum(m_old, jnp.max(top, axis=0, keepdims=True))
            m_st[b] = m
            alpha = jnp.exp2(m_old - m)
            top, o = None, None
            for c in range(chunks):
                if i + 1 < len(order):
                    top = scores(order[i + 1], c, nxt, top)
                x = cur[c * KB : (c + 1) * KB, :].reshape(KB // 8, 8, QB) - m[None]
                p = jnp.exp2(x).reshape(KB, QB).astype(jnp.bfloat16)
                term = jnp.dot(v_t[:, c * KB : (c + 1) * KB], p, preferred_element_type=jnp.float32)
                o = term if o is None else o + term
            o = acc[b] * alpha[0:1] + o
            if done is None:
                acc[b] = o
            else:
                done(b, o)

    def pair_sweep(step, order, which, kv):
        if which is not None:
            for k, places in enumerate(PAIRS):
                @pl.when(step == k)
                def _(k=k, places=places):
                    for place in places:
                        if place != (0, 0):
                            arrived(place, which, kv)
                            pass_on(place, which, kv)

        ids = [pick(step, [slot_of(places[i]) for places in PAIRS]) for i in range(2)]

        def tile_at(t):
            return kv[ids[t // tiles], t % tiles * TILE : (t % tiles + 1) * TILE, :]

        for t in range(2 * tiles):
            v_t[:HD, t * TILE : (t + 1) * TILE] = tile_at(t).T[HD:]
        per = KB // TILE
        sweep(
            lambda c: jnp.concatenate([tile_at(c * per + i) for i in range(per)], axis=0),
            2 * share, order, False, None,
        )

    v_t[HD:, :] = jnp.ones((v_t.shape[0] - HD, v_t.shape[1]), jnp.bfloat16)
    acc[...] = jnp.zeros_like(acc)
    m_st[...] = jnp.full(m_st.shape, -1e30, jnp.float32)

    first_half, second_half = list(range(n_half)), list(range(n_half, 2 * n_half))
    local[4].wait()
    local[5].wait()
    absorb_keys(latent[...], tp, 0, kv1, 0)
    lat[0].wait_recv()
    send_rows(4, raw.at[0, top], 2, top, right_tp)
    absorb_keys(raw[0, top, :], left_tp, 0, kv1, rows)
    lat[1].wait_recv()
    absorb_keys(raw[1, top, :], right_tp, 0, kv1, rows + half)
    pass_on((0, 0), 0, kv1)
    local[6].wait()
    absorb_queries([(tp, 0, rows), (left_tp, 0, half), (right_tp, 0, half)], 0)

    last_rows = send(raw.at[1, low], raw.at[2, low], lat_send.at[5], lat_recv.at[5], {"tp": left_tp})

    def one(step, carry):
        @pl.when(step == 1)
        def _():
            lat[3].wait_recv()
            last_rows.start()

        pair_sweep(step, first_half, 0, kv1)
        return carry

    lax.fori_loop(0, len(PAIRS), one, 0)

    local[3].wait()
    x = key_value(modulated(context[...], 1))
    kv2[0, share : share + ctx_rows, :] = jnp.where(left, headed(x, kg), x).astype(jnp.bfloat16)
    lat[2].wait_recv()
    absorb_keys(raw[0, low, :], left_tp, half, kv2, 0)
    absorb_keys(raw[1, low, :], right_tp, half, kv2, half)
    lat[4].wait_recv()
    last_rows.wait_recv()
    absorb_keys(raw[2], far_tp, 0, kv2, rows)
    pass_on((0, 0), 1, kv2)
    absorb_queries([(left_tp, half, half), (right_tp, half, half), (far_tp, 0, rows)], n_half)

    def two(step, carry):
        pair_sweep(step, second_half, None, kv1)
        return carry

    lax.fori_loop(0, len(PAIRS), two, 0)

    def three(step, carry):
        pair_sweep(step, first_half + second_half, 1, kv2)
        return carry

    lax.fori_loop(0, len(PAIRS), three, 0)

    def done(b, o):
        o = (o[:HD] / o[HD : HD + 1]).astype(jnp.bfloat16).astype(jnp.float32)
        both = jnp.concatenate([o[:, :TILE], o[:, TILE:]], axis=0)
        pair, tile = b % n_half // tiles, b % n_half % tiles
        at = b // n_half * share + tile * TILE
        o_tok[at : at + TILE, pair * 2 * HD : (pair + 1) * 2 * HD] = both.T.astype(jnp.bfloat16)

    for slot in range(n_sp):
        kv_ctx[slot * ctx_rows : (slot + 1) * ctx_rows, :] = kv2[slot, share:, :]
    n_ctx = n_sp * ctx_rows
    for t in range(n_ctx // TILE):
        v_t[:HD, t * TILE : (t + 1) * TILE] = kv_ctx[t * TILE : (t + 1) * TILE, :].T[HD:]
    sweep(lambda c: kv_ctx[c * KB : (c + 1) * KB, :], n_ctx, second_half + first_half, True, done)

    span = group * HD
    mine = pl.ds(pl.multiple_of(tp * span, span), span)
    o_copies = []
    for i, (at, count, owner, start) in enumerate(
        (
            (share + rows, rows, far_tp, 0),
            (share, half, left_tp, half),
            (share + half, half, right_tp, half),
            (rows, half, left_tp, 0),
            (rows + half, half, right_tp, 0),
        )
    ):
        copy = send(
            o_tok.at[at : at + count], o_all.at[start : start + count, mine],
            o_ssem.at[i], o_rsem.at[i], {"tp": owner},
        )
        copy.start()
        o_copies.append(copy)
    o_all[:, mine] = o_tok[0:rows, :]
    local[7].wait()
    for copy in o_copies:
        copy.wait_recv()

    for j in range(n_tp):
        cols = pl.ds(j * chunk, chunk)
        y_j = jnp.dot(o_all[...], wout[:, cols], preferred_element_type=jnp.float32)
        gate = mods_all[j, 4:5, :]
        out[:, cols] = (latent[:, cols].astype(jnp.float32) + gate * y_j).astype(jnp.bfloat16)

    for copy in lat + [last_rows] + pa + pb + o_copies:
        copy.wait_send()
    for index in range(len(flights)):
        flight(index, 0, kv1).wait_send()
        flight(index, 1, kv2).wait_send()


def on_device(n_sp, n_tp, latent, cond, cond_ctx, context, norm_gain, mod_shift, mod_scale, mod_gate,
              w_query, w_key, w_value, q_gain, k_gain, ctx_lift, w_out):
    _, rows, width = latent.shape
    tokens = rows * n_tp
    ctx_rows = context.shape[1]
    group = w_query.shape[1] // w_key.shape[1]
    keys = tokens + ctx_rows
    row_tab, col_tab = rope_tables(tokens * n_sp // GRID_W)
    chunk = mod_shift.shape[1]
    share = tokens // 2
    n_q = tokens // TILE * group // 2
    bf, f32 = jnp.bfloat16, jnp.float32
    vmem = pl.BlockSpec(memory_space=pltpu.VMEM)
    smem = pl.BlockSpec(memory_space=pltpu.SMEM)
    hbm = pl.BlockSpec(memory_space=pl.ANY)
    dma = pltpu.SemaphoreType.DMA
    out = pl.pallas_call(
        functools.partial(kernel, n_sp, n_tp, group),
        out_shape=jax.ShapeDtypeStruct((rows, width), bf),
        in_specs=[vmem] * 6 + [smem] + [vmem] * 2 + [hbm] * 8,
        out_specs=vmem,
        scratch_shapes=[
            pltpu.VMEM((ctx_rows, width), bf),
            pltpu.VMEM((3,) + mod_shift.shape, bf),
            pltpu.VMEM(w_query.shape, bf),
            pltpu.VMEM((2 * HD, width), bf),
            pltpu.VMEM(w_out.shape, bf),
            pltpu.VMEM((n_tp - 1, rows, width), bf),
            pltpu.VMEM((8, chunk), f32),
            pltpu.VMEM((n_sp - 1, 8, chunk), f32),
            pltpu.VMEM((n_tp, 8, chunk), f32),
            pltpu.VMEM((8, width), f32),
            pltpu.VMEM((2, tokens, 2 * HD), f32),
            pltpu.VMEM((share, width), bf),
            pltpu.VMEM((n_q, 4 * HD, QB), bf),
            pltpu.VMEM((n_sp, share, 2 * HD), bf),
            pltpu.VMEM((n_sp, share + ctx_rows, 2 * HD), bf),
            pltpu.VMEM((n_sp * ctx_rows, 2 * HD), bf),
            pltpu.VMEM((HD + 16, tokens), bf),
            pltpu.VMEM((tokens, QB), f32),
            pltpu.VMEM((tokens, QB), f32),
            pltpu.VMEM((n_q, HD + 16, QB), f32),
            pltpu.VMEM((n_q, 8, QB), f32),
            pltpu.VMEM((tokens, group * HD), bf),
            pltpu.VMEM((rows, n_tp * group * HD), bf),
            dma((8,)),
            dma((6,)), dma((6,)),
            dma((n_sp - 1,)), dma((n_sp - 1,)),
            dma((n_tp - 1,)), dma((n_tp - 1,)),
            dma((2, n_sp - 1)), dma((2, n_sp)),
            dma((5,)), dma((5,)),
        ],
        compiler_params=pltpu.CompilerParams(
            collective_id=0, has_side_effects=True, vmem_limit_bytes=60 * 1024 * 1024
        ),
    )(
        latent[0], cond, cond_ctx[None], norm_gain.reshape(width // TILE, TILE), q_gain[None], k_gain[None], ctx_lift,
        jnp.asarray(row_tab), jnp.asarray(col_tab),
        context[0], mod_shift, mod_scale, mod_gate, w_query, w_key.T, w_value.T, w_out,
    )
    return out[None]


def solution(mesh):
    placed = (
        P("dp", ("sp", "tp"), None),
        P("dp", "sp"),
        P("sp"),
        P("dp", "sp", None),
        P(),
        P("sp", "tp"),
        P("sp", "tp"),
        P("sp", "tp"),
        P(None, "tp"),
        P(None, "tp"),
        P(None, "tp"),
        P(),
        P(),
        P("tp"),
        P(),
    )
    return jax.shard_map(
        functools.partial(on_device, mesh.shape["sp"], mesh.shape["tp"]),
        mesh=mesh,
        in_specs=placed,
        out_specs=P("dp", ("sp", "tp"), None),
        check_vma=False,
    )
```

time: 143 us -> 96.7 us (0.68)
  Pallas kernels: 134 us -> 94.4 us
  local copies, waits for them, and re-layouts: 7.29 us -> 2.09 us
    pallas_call x1, Pallas kernels: 134 us -> 94.4 us  [on_device(): pl.pallas_call(functools.partial(kernel, n_sp, n_tp, group), out_shape=ja...]
    unnamed x3 -> x1, local copies, waits for them, and re-layouts: 6 us -> 2.09 us
where the time goes in v1:
time: 96.7 us; the launch traced here: 96.5 us
  Pallas kernels  94.4 us (98%)
  local copies, waits for them, and re-layouts  2.09 us (2%)
    pallas_call x1, Pallas kernels, on_device(): pl.pallas_call(functools.partial(kernel, n_sp, n_tp, group), out_shape=ja...  94.4 us
    unnamed x1, local copies, waits for them, and re-layouts  2.09 us

profile of v1, /device:TPU:0, one launch (start us, length us, event | category | flops | bytes accessed | tf_op | source)
XLA Modules:
  0.0 96.5 jit_solution(8932189823666971937)
XLA Ops:
  0.0 94.4 %shard_map.163 = bf16[192,2048]{1,0:T(8,128)(2,1)} custom-call(bf16[192,2048]{1,0:T(8,128)(2,1)} %bitcast.10, bf16[1,128]{1,0:T(2,128)(2,1)} %cond.1, bf16[1,128]{1,0:T(2,128)(2,1)} %bitcast.15, bf16[16,128]{1,0:T(8,128)(2,1)} %bitcast.14, bf16[1,64]{1,0:T(2,128)(2,1)} %bitcast.16, bf16[1,64]{1,0:T(2,128)(2,1)} %bitcast.17, f32[4]{0:T(128)} %lift.1, ...), custom_call_target="tpu_custom_call" | custom-call | tf_op jit(solution)/shard_map/pallas_call | solution.py:449
  94.4 2.1 %copy.19 = bf16[1,192,2048]{2,1,0:T(8,128)(2,1)} copy(bf16[1,192,2048]{2,1,0:T(8,128)(2,1)} %bitcast.9) | data formatting | bytes 1572864
